TPU v7x, 32 devices: a whole 2x2x4 slice. The times are simulated.
32 devices in a mesh: ep: 8 (over z, x), tp: 4 (over y, core).
Axes of the slice: x: 2, y: 2, z: 4, core: 2. Of those that a mesh axis runs over, the one named last changes fastest.
Arguments:
- tokens: bfloat16 [512, 2048], P('ep'), may hold values from -6 to 6
- norm_gain: float32 [2048], replicated, may hold values from 0.1 to 1.9
- norm_shift: float32 [2048], replicated, may hold values from -3 to 3
- expert_ids: int32 [512, 4], P('ep'), may hold values from 0 to 15, as said below
- gate_weights: float32 [512, 4], P('ep'), may hold values from 0.1 to 1
- expert_gate: bfloat16 [16, 2048, 512], P('ep', None, 'tp'), may hold values from -0.125 to 0.125
- expert_up: bfloat16 [16, 2048, 512], P('ep', None, 'tp'), may hold values from -0.125 to 0.125
- expert_down: bfloat16 [16, 512, 2048], P('ep', 'tp'), may hold values from -0.25 to 0.25
Outputs:
- mixed_out: bfloat16 [512, 2048], P('ep', 'tp')
Inputs may be any that keep to these rules, and one draw needn't show every extreme that they name: `expert_ids`: each row names 4 distinct experts that all lie in one group of 4 consecutive expert numbers. In the rows of one index of ep (aligned blocks of 64 rows) no expert is named by more than 32 rows, and in every block some expert is named by exactly 32 rows.
All inputs are finite; a program needn't handle non-finite values.
Results may differ from a plain program's by a relative error of at most 0.002.
Values may be sent and summed in bfloat16 or wider, within the bound.
A program may use at most 64 MiB of HBM per device.

v0:
```python
import jax
import jax.numpy as jnp
from jax import lax
from jax.sharding import PartitionSpec as P

GROUPS = 4


epsilon = 1e-05


def layer_norm(tokens, norm_gain, norm_shift):
    values = tokens.astype(jnp.float32)
    centre = jnp.mean(values, axis=-1, keepdims=True)
    spread = jnp.mean(jnp.square(values - centre), axis=-1, keepdims=True)
    scaled = (values - centre) * lax.rsqrt(spread + epsilon) * norm_gain + norm_shift
    return scaled.astype(jnp.bfloat16)


def per_device(
    tokens, norm_gain, norm_shift, expert_ids, gate_weights, expert_gate, expert_up, expert_down
):
    tok_rows, features = tokens.shape
    top_count = expert_ids.shape[1]
    local_count = expert_gate.shape[0]
    ep_size = lax.axis_size("ep")
    total_experts = local_count * ep_size
    group_size = total_experts // GROUPS
    capacity = tok_rows // 2 * top_count // group_size
    recv_rows = ep_size * capacity
    normed = layer_norm(tokens, norm_gain, norm_shift)
    flat_ids = expert_ids.reshape(-1)
    onehot = (flat_ids[:, None] == jnp.arange(total_experts, dtype=jnp.int32)[None, :]).astype(
        jnp.int32
    )
    before = jnp.cumsum(onehot, axis=0) - onehot
    slot_index = jnp.sum(before * onehot, axis=1)
    positions = flat_ids * capacity + slot_index
    source_rows = jnp.repeat(normed, top_count, axis=0)
    packed = (
        jnp.zeros((total_experts * capacity, features), jnp.bfloat16).at[positions].set(source_rows)
    )

    def to_experts(received):
        columns = received.shape[-1]
        arranged = received.reshape(ep_size, local_count, capacity, columns).transpose(1, 0, 2, 3)
        return arranged.reshape(local_count, recv_rows, columns)

    def to_sources(result):
        columns = result.shape[-1]
        arranged = result.reshape(local_count, ep_size, capacity, columns).transpose(1, 0, 2, 3)
        return arranged.reshape(total_experts * capacity, columns)

    arrived = to_experts(lax.all_to_all(packed, "ep", split_axis=0, concat_axis=0, tiled=True))
    gate_sum = jnp.einsum("erd,edf->erf", arrived, expert_gate, preferred_element_type=jnp.float32)
    upward = jnp.einsum("erd,edf->erf", arrived, expert_up, preferred_element_type=jnp.float32)
    hidden = (jax.nn.silu(gate_sum) * upward).astype(jnp.bfloat16)
    partial_out = jnp.einsum(
        "erf,efd->erd", hidden, expert_down, preferred_element_type=jnp.float32
    )
    weights_flat = gate_weights.reshape(-1)

    def combine(returned):
        picked = returned[positions] * weights_flat[:, None]
        return jnp.sum(picked.reshape(tok_rows, top_count, picked.shape[-1]), axis=1)

    reduced = lax.psum_scatter(partial_out, "tp", scatter_dimension=2, tiled=True)
    returned = lax.all_to_all(to_sources(reduced), "ep", split_axis=0, concat_axis=0, tiled=True)
    mixed_out = combine(returned)
    return mixed_out.astype(jnp.bfloat16)


def solution(mesh):
    return jax.shard_map(
        per_device,
        mesh=mesh,
        in_specs=(
            P("ep", None),
            P(),
            P(),
            P("ep", None),
            P("ep", None),
            P("ep", None, "tp"),
            P("ep", None, "tp"),
            P("ep", "tp", None),
        ),
        out_specs=P("ep", "tp"),
        check_vma=False,
    )
```

profile of v0, /device:TPU:0, one launch (start us, length us, event | category | flops | bytes accessed | tf_op | source)
XLA Modules:
  0.0 168.3 jit_solution(3622608224932434658)
XLA Ops:
  6.5 0.0 copy-start
  6.5 0.0 reduce-scatter.2.cloned.1.call-start
  6.5 0.9 copy.11
  7.4 0.1 eq.29
  7.5 0.1 eq.25
  7.6 0.7 broadcast_multiply_fusion
  8.3 0.6 reduce-window.6
  8.9 0.2 slice_reduce_fusion
  9.1 0.1 copy.10
  9.2 0.1 mul.53
  9.3 1.1 convert_reduce_fusion
  10.4 1.2 fusion.6
  11.6 1.1 fusion.9
  12.8 0.5 broadcast_in_dim.5
  13.3 1.1 reshape.104
  14.4 0.1 fusion.18
  14.5 3.5 %scatter_custom_fusion = bf16[512,2048]{1,0:T(8,128)(2,1)S(1)} fusion(s32[256]{0:T(256)S(1)} %bitcast.42, bf16[256,2048]{1,0:T(8,128)(2,1)} %reshape.104, bf16[]{:T(256)} %constant.8.clone.1), kind=kCustom, calls=%fused_computation.5 | custom fusion | bytes 2097664 | tf_op jit(solution)/shard_map/scatter | solution.py:41
  18.0 55.8 %all_to_all.21 = bf16[8,64,2048]{2,1,0:T(8,128)(2,1)S(1)} all-to-all(bf16[8,64,2048]{2,1,0:T(8,128)(2,1)S(1)} %bitcast.39), channel_id=1, replica_groups=mesh['ep'=8,'tp'=4] {'ep'}, dimensions={0} | all-to-all | bytes 4194304 | tf_op jit(solution)/shard_map/all_to_all | solution.py:54
  73.8 0.0 copy-start.1
  73.8 0.1 copy.14
  73.9 1.1 copy-done.1
  75.0 0.7 fusion.21
  75.7 0.0 copy-done
  75.7 4.4 %fusion.1 = f32[2,256,2048]{2,1,0:T(8,128)} fusion(bf16[2,128,2048]{2,1,0:T(8,128)(2,1)S(1)} %copy-done, bf16[2,256,2048]{2,1,0:T(8,128)(2,1)S(1)} %bitcast.38, bf16[2,2048,128]{2,1,0:T(8,128)(2,1)} %param.14, f32[2,256,128]{2,1,0:T(8,128)S(1)} %fusion.21), kind=kOutput, calls=%fused_computation.4 | convolution fusion | flops 537264128 | bytes 8650752 | tf_op jit(solution)/shard_map/erf,efd->erd/dot_general | solution.py:58
  80.1 0.0 reduce-scatter.2.cloned.1.call-update
  80.2 45.5 %reduce-scatter.2.cloned.1.call-done = f32[2,256,512]{2,1,0:T(8,128)} async-done(((f32[2,256,2048]{2,1,0:T(8,128)}), f32[2,256,512]{2,1,0:T(8,128)}) %reduce-scatter.2.cloned.1.call-update) | async-done | bytes 1048592 | tf_op jit(solution)/shard_map/reduce_scatter | solution.py:67
  125.7 0.0 copy-start.2
  125.7 2.3 %copy.15 = f32[2,8,32,512]{3,2,0,1:T(8,128)} copy(f32[2,8,32,512]{3,2,1,0:T(8,128)} %bitcast.41) | data formatting | bytes 2097152 | tf_op jit(solution)/shard_map/reshape | solution.py:51
  128.0 5.5 %all-to-all-start.1 = ((f32[8,64,512]{2,1,0:T(8,128)}), f32[8,64,512]{2,1,0:T(8,128)S(1)}, u32[]{:S(2)}, u32[]{:S(2)}) async-start(f32[8,64,512]{2,1,0:T(8,128)} %bitcast.9), calls=%async_computation.2 | async-start | bytes 2097152 | tf_op jit(solution)/shard_map/all_to_all | solution.py:68
  133.5 0.0 copy-done.2
  133.5 0.1 copy.16
  133.6 25.7 %all-to-all-done.1 = f32[8,64,512]{2,1,0:T(8,128)S(1)} async-done(((f32[8,64,512]{2,1,0:T(8,128)}), f32[8,64,512]{2,1,0:T(8,128)S(1)}, u32[]{:S(2)}, u32[]{:S(2)}) %all-to-all-start.1) | async-done | bytes 1048608 | tf_op jit(solution)/shard_map/all_to_all | solution.py:68
  159.4 1.0 gather_fusion
  160.3 0.1 gather.6
  160.5 1.0 multiply_reduce_fusion
  (7 shorter events, 0.1 us)
Async XLA Ops:
  6.5 69.2 %copy-start = (bf16[2,128,2048]{2,1,0:T(8,128)(2,1)S(1)}, bf16[2,128,2048]{2,1,0:T(8,128)(2,1)}, u32[]{:S(2)}) copy-start(bf16[2,128,2048]{2,1,0:T(8,128)(2,1)} %param.15) | copy-start | bytes 3145732
  6.5 119.1 %reduce-scatter.2.cloned.1.call-start = ((), (), s32[]{:S(2)}) async-start(), calls=%async_computation.3 | async-start | bytes 5242880 | tf_op jit(solution)/shard_map/reduce_scatter | solution.py:67
  73.8 1.2 copy-start.1
  125.7 7.8 %copy-start.2 = (f32[64,4]{0,1:T(4,128)S(1)}, f32[64,4]{0,1:T(4,128)}, u32[]{:S(2)}) copy-start(f32[64,4]{0,1:T(4,128)} %param.12) | copy-start | bytes 3076
  128.0 31.4 %all-to-all-start.1 = ((f32[8,64,512]{2,1,0:T(8,128)}), f32[8,64,512]{2,1,0:T(8,128)S(1)}, u32[]{:S(2)}, u32[]{:S(2)}) async-start(f32[8,64,512]{2,1,0:T(8,128)} %bitcast.9), calls=%async_computation.2 | async-start | bytes 2097152 | tf_op jit(solution)/shard_map/all_to_all | solution.py:68
Sparse Core Ops, SparseCore 0:
  80.3 45.3 reduce-scatter.1
where the time goes:
time: 169 us; the launch traced here: 168 us
  waiting for transfers between devices  71.3 us (42%)
  blocking collectives  55.8 us (33%)
  between operations  13.5 us (8%)
  local copies, waits for them, and re-layouts  11.4 us (7%)
  other arithmetic  5.87 us (3%)
  starting transfers between devices  5.5 us (3%)
  matrix products  5.1 us (3%)
    all_to_all x1, blocking collectives, per_device(): lax.all_to_all(packed, 'ep', split_axis=0, concat_axis=0, tiled=True)  55.8 us
    reduce_scatter x1, waiting for transfers between devices, per_device(): lax.psum_scatter(partial_out, 'tp', scatter_dimension=2, tiled=True)  45.5 us
    all_to_all x1, waiting for transfers between devices, per_device(): lax.all_to_all(to_sources(reduced), 'ep', split_axis=0, concat_axis=0, ti...  25.7 us
    all_to_all x1, starting transfers between devices, per_device(): lax.all_to_all(to_sources(reduced), 'ep', split_axis=0, concat_axis=0, ti...  5.5 us
    dot_general x1, matrix products, per_device(): jnp.einsum('erf,efd->erd', hidden, expert_down, preferred_element_type=jn...  4.39 us
    scatter x1, local copies, waits for them, and re-layouts, per_device(): jnp.zeros((total_experts * capacity, features), jnp.bfloat16).at[positions]  3.5 us
  transfers between devices with their start and end apart: 2, of which 2 were waited for; matrix products, arithmetic and copies ran while one was open for 0% of the time, Pallas kernels for 0%

commit v1 on v0

v1 whole, which is shorter than its diff:
```python
import functools

import jax
import jax.numpy as jnp
from jax import lax
from jax.experimental import pallas as pl
from jax.experimental.pallas import tpu as pltpu
from jax.sharding import PartitionSpec as P

GROUPS = 4
CORES = 2
EPSILON = 1e-05
MESH = pl.DeviceIdType.MESH


def kernel(
    ep_size, tp_size,
    tok_ref, gain_ref, shift_ref, ids_ref, gw_ref, wg_ref, wu_ref, wd_ref, out_ref,
    x_buf, xs_buf, sel_buf, wall_buf, wr_buf, wcat, wdn, acc,
    r1_send, r1_recv, r1_own, r2_send, r2_recv, f_send, f_recv,
    w_sem, s1_s, s1_r, wt_s, wt_r, a_s, a_r, b_s, b_r, c1_s, c1_r, c2_s, c2_r, c3_s, c3_r,
):
    tok_rows, features = tok_ref.shape
    local, _, units = wg_ref.shape
    top_k = ids_ref.shape[1]
    members = ep_size // GROUPS
    rows_tp = tp_size // CORES
    group_size = local * members
    half = tok_rows // 2
    quarter = features // tp_size
    lanes = GROUPS * half
    parts, _, width = wcat.shape

    e = lax.axis_index("ep")
    j = lax.axis_index("tp")
    gme, m = e // members, e % members
    y, c = j // CORES, j % CORES
    partner = {"ep": e, "tp": y * CORES + (1 - c)}
    others = [(dm, dy) for dm in range(members) for dy in range(rows_tp) if dm or dy]
    slots = others + [(0, 0)]
    own = len(others)

    def ahead(k):
        dm, dy = slots[k]
        return lax.rem(m + dm, members), lax.rem(y + dy, rows_tp)

    def behind(k):
        dm, dy = slots[k]
        return lax.rem(m + members - dm, members), lax.rem(y + rows_tp - dy, rows_tp)

    def block_at(db):
        return lax.rem(gme + GROUPS - db, GROUPS)

    def remote(src, dst, ssem, rsem, dev):
        return pltpu.make_async_remote_copy(
            src_ref=src, dst_ref=dst, send_sem=ssem, recv_sem=rsem,
            device_id=dev, device_id_type=MESH,
        )

    sent = []

    def start(*args):
        copy = remote(*args)
        copy.start()
        sent.append(copy)

    barrier = pltpu.get_barrier_semaphore()
    greeted = 0
    for d in range(1, ep_size):
        pl.semaphore_signal(
            barrier, inc=1, device_id={"ep": lax.rem(e + d, ep_size), "tp": j}, device_id_type=MESH
        )
        greeted += 1
    for k, (dm, dy) in enumerate(others):
        if dy:
            mm, yy = ahead(k)
            pl.semaphore_signal(
                barrier, inc=1,
                device_id={"ep": gme * members + mm, "tp": yy * CORES + c}, device_id_type=MESH,
            )
            greeted += 1
    pl.semaphore_signal(barrier, inc=1, device_id=partner, device_id_type=MESH)
    greeted += 1

    weights = []
    for le in range(local):
        for source, at in ((wg_ref, 2 * le * units), (wu_ref, (2 * le + 1) * units)):
            weights.append(
                (source.at[le], wcat.at[at // width, :, pl.ds(at % width, units)])
            )
        for q in range(tp_size):
            weights.append((wd_ref.at[le, :, pl.ds(q * quarter, quarter)], wdn.at[q, le]))
    weights = [pltpu.make_async_copy(s, d, w_sem.at[i]) for i, (s, d) in enumerate(weights)]
    for copy in weights:
        copy.start()

    ids = ids_ref[...]
    group_of = ids[:, 0:1] // group_size
    lane = lax.broadcasted_iota(jnp.int32, (tok_rows, lanes), 1)
    in_group = group_of == lane // half
    earlier = (
        lax.broadcasted_iota(jnp.int32, (tok_rows, tok_rows), 1)
        < lax.broadcasted_iota(jnp.int32, (tok_rows, tok_rows), 0)
    )
    rank = jnp.dot(
        earlier.astype(jnp.float32).astype(jnp.bfloat16),
        in_group.astype(jnp.float32).astype(jnp.bfloat16),
        preferred_element_type=jnp.float32,
    )
    picked = in_group & (rank == (lane % half).astype(jnp.float32))
    sel = picked.astype(jnp.float32)
    sel_bf = sel.astype(jnp.bfloat16)
    sel_buf[...] = sel_bf
    within = ids - group_of * group_size
    gw = gw_ref[...]
    wall_buf[...] = jnp.zeros_like(wall_buf)
    for i in range(group_size):
        mine = jnp.sum(jnp.where(within == i, gw, 0.0), axis=1, keepdims=True)
        wall_buf[i : i + 1, :] = jnp.sum(sel * mine, axis=0, keepdims=True)

    values = tok_ref[...].astype(jnp.float32)
    centre = jnp.mean(values, axis=-1, keepdims=True)
    spread = jnp.mean(jnp.square(values - centre), axis=-1, keepdims=True)
    share = pl.ds(pl.multiple_of(j * quarter, quarter), quarter)
    part = tok_ref[:, share].astype(jnp.float32)
    normed = (
        (part - centre) * lax.rsqrt(spread + EPSILON) * gain_ref[:, share] + shift_ref[:, share]
    ).astype(jnp.bfloat16)
    packed = lax.dot_general(
        sel_bf, normed, (((0,), (0,)), ((), ())), preferred_element_type=jnp.float32
    ).astype(jnp.bfloat16)
    packed = packed.reshape(GROUPS, half, quarter)
    xs_buf[...] = packed

    pl.semaphore_wait(barrier, greeted)

    for dg in range(1, GROUPS):
        g = lax.rem(gme + dg, GROUPS)
        start(
            xs_buf.at[g], x_buf.at[m, j, gme], s1_s.at[dg], s1_r.at[dg],
            {"ep": g * members + m, "tp": j},
        )
    x_buf[m, j, gme] = xs_buf[gme]
    for d in range(1, ep_size):
        start(
            wall_buf, wr_buf.at[e], wt_s.at[d], wt_r.at[d],
            {"ep": lax.rem(e + d, ep_size), "tp": j},
        )
    wr_buf[e] = wall_buf[...]

    for db in range(GROUPS):
        b = block_at(db)
        mine = x_buf.at[m, j, b]
        if db:
            remote(mine, mine, s1_s.at[db], s1_r.at[db], partner).wait_recv()
        for k in range(own):
            mm, yy = ahead(k)
            start(
                mine, mine, a_s.at[db, k], a_r.at[db, k],
                {"ep": gme * members + mm, "tp": yy * CORES + c},
            )
        start(mine, mine, b_s.at[db, own], b_r.at[db, own], partner)
    for db in range(GROUPS):
        b = block_at(db)
        for k in range(own):
            mm, yy = behind(k)
            slot = x_buf.at[mm, yy * CORES + c, b]
            remote(slot, slot, a_s.at[db, k], a_r.at[db, k], partner).wait_recv()
            start(slot, slot, b_s.at[db, k], b_r.at[db, k], partner)

    for copy in weights:
        copy.wait()
    acc[...] = jnp.zeros_like(acc)

    def project(mm, jj):
        rows = x_buf[mm, jj].reshape(lanes, quarter)
        depth = pl.ds(pl.multiple_of(jj * quarter, quarter), quarter)
        for part in range(parts):
            acc[mm, part] += jnp.dot(
                rows, wcat[part, depth, :], preferred_element_type=jnp.float32
            )

    order = [own] + list(range(own))
    for k in order:
        mm, yy = behind(k)
        project(mm, yy * CORES + c)
    for d in range(1, ep_size):
        slot = wr_buf.at[lax.rem(e + ep_size - d, ep_size)]
        remote(slot, slot, wt_s.at[d], wt_r.at[d], partner).wait_recv()
    for k in order:
        mm, yy = behind(k)
        for db in range(GROUPS):
            slot = x_buf.at[mm, yy * CORES + (1 - c), block_at(db)]
            remote(slot, slot, b_s.at[db, k], b_r.at[db, k], partner).wait_recv()
        project(mm, yy * CORES + (1 - c))

    slot_row = lax.broadcasted_iota(jnp.int32, (half, lanes), 0) + gme * half
    slot_lane = lax.broadcasted_iota(jnp.int32, (half, lanes), 1)
    diagonal = slot_row == slot_lane
    hidden, scale = {}, {}
    for dm in range(members):
        mm = lax.rem(m + dm, members)
        for le in range(local):
            at, to = 2 * le * units, (2 * le + 1) * units
            gate = acc[mm, at // width, :, at % width : at % width + units]
            up = acc[mm, to // width, :, to % width : to % width + units]
            hidden[dm, le] = (gate / (1.0 + jnp.exp(-gate)) * up).astype(jnp.bfloat16)
            columns = []
            for b in range(GROUPS):
                row = wr_buf[b * members + mm, pl.ds(m * local + le, 1), :]
                columns.append(jnp.sum(jnp.where(diagonal, row, 0.0), axis=1, keepdims=True))
            scale[dm, le] = jnp.concatenate(columns, axis=0)

    def lower(dm, q):
        total = None
        for le in range(local):
            term = scale[dm, le] * jnp.dot(
                hidden[dm, le], wdn[q, le], preferred_element_type=jnp.float32
            )
            total = term if total is None else total + term
        return total

    for k in range(own + 1):
        _, yy = ahead(k)
        r1_send[k] = lower(slots[k][0], yy * CORES + (1 - c))
        start(r1_send.at[k], r1_recv.at[k], c1_s.at[k], c1_r.at[k], partner)
    for k in range(own + 1):
        _, yy = ahead(k)
        r1_own[k] = lower(slots[k][0], yy * CORES + c)
    for k in range(own + 1):
        mm, yy = ahead(k)
        slot = r1_recv.at[k]
        remote(slot, slot, c1_s.at[k], c1_r.at[k], partner).wait_recv()
        summed = r1_own[k] + r1_recv[k]
        if k < own:
            r2_send[k] = summed
            start(
                r2_send.at[k], r2_recv.at[k], c2_s.at[k], c2_r.at[k],
                {"ep": gme * members + mm, "tp": yy * CORES + c},
            )
    for k in range(own):
        slot = r2_recv.at[k]
        remote(slot, slot, c2_s.at[k], c2_r.at[k], partner).wait_recv()
        summed = summed + r2_recv[k]
    f_send[...] = summed.astype(jnp.bfloat16).reshape(GROUPS, half, quarter)
    for dg in range(1, GROUPS):
        g = lax.rem(gme + dg, GROUPS)
        start(
            f_send.at[g], f_recv.at[gme], c3_s.at[dg], c3_r.at[dg],
            {"ep": g * members + m, "tp": j},
        )
    f_recv[gme] = f_send[gme]
    for dg in range(1, GROUPS):
        slot = f_recv.at[block_at(dg)]
        remote(slot, slot, c3_s.at[dg], c3_r.at[dg], partner).wait_recv()
    out_ref[...] = jnp.dot(
        sel_buf[...], f_recv[...].reshape(lanes, quarter), preferred_element_type=jnp.float32
    ).astype(jnp.bfloat16)
    for copy in sent:
        copy.wait_send()


def per_device(tokens, norm_gain, norm_shift, expert_ids, gate_weights, w_gate, w_up, w_down):
    ep_size, tp_size = lax.axis_size("ep"), lax.axis_size("tp")
    tok_rows, features = tokens.shape
    local, _, units = w_gate.shape
    members, rows_tp = ep_size // GROUPS, tp_size // CORES
    half, quarter = tok_rows // 2, features // tp_size
    lanes = GROUPS * half
    group_size = local * members
    padded = -(-group_size // 8) * 8
    chunks = members * rows_tp
    parts, width = (1, 2 * local * units) if units % 128 == 0 else (2 * local, units)
    bf16, f32 = jnp.bfloat16, jnp.float32
    dma = pltpu.SemaphoreType.DMA
    vmem = pl.BlockSpec(memory_space=pltpu.VMEM)
    hbm = pl.BlockSpec(memory_space=pl.ANY)
    return pl.pallas_call(
        functools.partial(kernel, ep_size, tp_size),
        out_shape=jax.ShapeDtypeStruct((tok_rows, quarter), bf16),
        in_specs=[vmem] * 5 + [hbm] * 3,
        out_specs=vmem,
        scratch_shapes=[
            pltpu.VMEM((members, tp_size, GROUPS, half, quarter), bf16),
            pltpu.VMEM((GROUPS, half, quarter), bf16),
            pltpu.VMEM((tok_rows, lanes), bf16),
            pltpu.VMEM((padded, lanes), f32),
            pltpu.VMEM((ep_size, padded, lanes), f32),
            pltpu.VMEM((parts, features, width), bf16),
            pltpu.VMEM((tp_size, local, units, quarter), bf16),
            pltpu.VMEM((members, parts, lanes, width), f32),
            pltpu.VMEM((chunks, lanes, quarter), f32),
            pltpu.VMEM((chunks, lanes, quarter), f32),
            pltpu.VMEM((chunks, lanes, quarter), f32),
            pltpu.VMEM((chunks, lanes, quarter), f32),
            pltpu.VMEM((chunks, lanes, quarter), f32),
            pltpu.VMEM((GROUPS, half, quarter), bf16),
            pltpu.VMEM((GROUPS, half, quarter), bf16),
            dma((local * (2 + tp_size),)),
            dma((GROUPS,)), dma((GROUPS,)),
            dma((ep_size,)), dma((ep_size,)),
            dma((GROUPS, chunks)), dma((GROUPS, chunks)),
            dma((GROUPS, chunks)), dma((GROUPS, chunks)),
            dma((chunks,)), dma((chunks,)),
            dma((chunks,)), dma((chunks,)),
            dma((GROUPS,)), dma((GROUPS,)),
        ],
        compiler_params=pltpu.CompilerParams(
            collective_id=0, has_side_effects=True, vmem_limit_bytes=48 * 1024 * 1024
        ),
    )(
        tokens, norm_gain.reshape(1, features), norm_shift.reshape(1, features),
        expert_ids, gate_weights, w_gate, w_up, w_down,
    )


def solution(mesh):
    return jax.shard_map(
        per_device,
        mesh=mesh,
        in_specs=(
            P("ep", None),
            P(),
            P(),
            P("ep", None),
            P("ep", None),
            P("ep", None, "tp"),
            P("ep", None, "tp"),
            P("ep", "tp", None),
        ),
        out_specs=P("ep", "tp"),
        check_vma=False,
    )
```

time: 169 us -> 45.7 us (0.27)
  waiting for transfers between devices: 71.3 us -> 0 us
  blocking collectives: 55.8 us -> 0 us
  Pallas kernels: 0 us -> 38 us
  between operations: 13.5 us -> 0.02 us
  other arithmetic: 5.87 us -> 0 us
  starting transfers between devices: 5.5 us -> 0 us
  matrix products: 5.1 us -> 0 us
  local copies, waits for them, and re-layouts: 11.4 us -> 7.33 us
    all_to_all x1 -> x0, blocking collectives: 55.8 us -> none  [per_device(): lax.all_to_all(packed, 'ep', split_axis=0, concat_axis=0, tiled=True)]
    reduce_scatter x1 -> x0, waiting for transfers between devices: 45.5 us -> none  [per_device(): lax.psum_scatter(partial_out, 'tp', scatter_dimension=2, tiled=True)]
    pallas_call x0 -> x1, Pallas kernels: none -> 38 us  [per_device(): pl.pallas_call(functools.partial(kernel, ep_size, tp_size), out_shape=jax...]
    all_to_all x1 -> x0, waiting for transfers between devices: 25.7 us -> none  [per_device(): lax.all_to_all(to_sources(reduced), 'ep', split_axis=0, concat_axis=0, ti...]
    all_to_all x1 -> x0, starting transfers between devices: 5.5 us -> none  [per_device(): lax.all_to_all(to_sources(reduced), 'ep', split_axis=0, concat_axis=0, ti...]
    unnamed x8 -> x19, local copies, waits for them, and re-layouts: 2.05 us -> 7.33 us
    dot_general x2 -> x0, matrix products: 5.1 us -> none  [the longest x1 4.39 us: per_device(): jnp.einsum('erf,efd->erd', hidden, expert_down, preferred_element_type=jn...]
    scatter x1 -> x0, local copies, waits for them, and re-layouts: 3.5 us -> none  [per_device(): jnp.zeros((total_experts * capacity, features), jnp.bfloat16).at[positions]]
  transfers between devices with their start and end apart: 2 -> 0, of which waited for: 2 -> 0; matrix products, arithmetic and copies ran while one was open for 0% -> 0% of each run, Pallas kernels for 0% -> 0%
where the time goes in v1:
time: 45.7 us; the launch traced here: 45.3 us
  Pallas kernels  38 us (83%)
  local copies, waits for them, and re-layouts  7.33 us (16%)
    pallas_call x1, Pallas kernels, per_device(): pl.pallas_call(functools.partial(kernel, ep_size, tp_size), out_shape=jax...  38 us
    unnamed x19, local copies, waits for them, and re-layouts  7.33 us

profile of v1, /device:TPU:0, one launch (start us, length us, event | category | flops | bytes accessed | tf_op | source)
XLA Modules:
  0.0 45.3 jit_solution(8636351524202051146)
XLA Ops:
  0.0 0.0 copy-start.6
  0.0 0.7 %copy-done.6 = s32[64,4]{0,1:T(4,128)S(1)} copy-done((s32[64,4]{0,1:T(4,128)S(1)}, s32[64,4]{0,1:T(4,128)}, u32[]{:S(2)}) %copy-start.6) | copy-done | bytes 1048
  0.7 0.0 copy-start.7
  0.7 0.1 copy.9.ids_ref
  0.8 0.6 %copy-done.7 = f32[64,4]{0,1:T(4,128)S(1)} copy-done((f32[64,4]{0,1:T(4,128)S(1)}, f32[64,4]{0,1:T(4,128)}, u32[]{:S(2)}) %copy-start.7) | copy-done | bytes 1048
  1.4 0.0 copy-start.4
  1.4 0.0 copy-start.5
  1.4 0.1 copy.10.gw_ref
  1.5 0.6 %copy-done.4 = f32[2048]{0:T(1024)S(1)} copy-done((f32[2048]{0:T(1024)S(1)}, f32[2048]{0:T(1024)}, u32[]{:S(2)}) %copy-start.4) | copy-done | bytes 8216
  2.1 0.0 copy-done.5
  2.1 0.0 copy-start
  2.1 1.2 %copy-done = bf16[2,2048,128]{2,1,0:T(8,128)(2,1)S(1)} copy-done((bf16[2,2048,128]{2,1,0:T(8,128)(2,1)S(1)}, bf16[2,2048,128]{2,1,0:T(8,128)(2,1)}, u32[]{:S(2)}) %copy-start) | copy-done | bytes 1048600
  3.3 0.0 copy-start.1
  3.3 1.2 %copy-done.1 = bf16[2,2048,128]{2,1,0:T(8,128)(2,1)S(1)} copy-done((bf16[2,2048,128]{2,1,0:T(8,128)(2,1)S(1)}, bf16[2,2048,128]{2,1,0:T(8,128)(2,1)}, u32[]{:S(2)}) %copy-start.1) | copy-done | bytes 1048600
  4.5 0.0 copy-start.2
  4.5 1.2 %copy-done.2 = bf16[2,128,2048]{2,1,0:T(8,128)(2,1)S(1)} copy-done((bf16[2,128,2048]{2,1,0:T(8,128)(2,1)S(1)}, bf16[2,128,2048]{2,1,0:T(8,128)(2,1)}, u32[]{:S(2)}) %copy-start.2) | copy-done | bytes 1048600
  5.8 0.0 copy-start.3
  5.8 0.9 %copy-done.3 = bf16[64,2048]{1,0:T(8,128)(2,1)S(1)} copy-done((bf16[64,2048]{1,0:T(8,128)(2,1)S(1)}, bf16[64,2048]{1,0:T(8,128)(2,1)}, u32[]{:S(2)}) %copy-start.3) | copy-done | bytes 262168
  6.7 38.0 %shard_map.82 = bf16[64,512]{1,0:T(8,128)(2,1)S(1)} custom-call(bf16[64,2048]{1,0:T(8,128)(2,1)S(1)} %copy-done.3, f32[1,2048]{1,0:T(1,128)S(1)} %bitcast.2, f32[1,2048]{1,0:T(1,128)S(1)} %bitcast.3, s32[64,4]{1,0:T(8,128)S(1)} %copy.9.ids_ref, f32[64,4]{1,0:T(8,128)S(1)} %copy.10.gw_ref, bf16[2,2048,128]{2,1,0:T(8,128)(2,1)S(1)} %copy-done, ...), custom_call_target="tpu_custom_call" | custom-call | tf_op jit(solution)/shard_map/pallas_call | solution.py:278
  44.7 0.6 %copy.12 = bf16[64,512]{1,0:T(8,128)(2,1)} copy(bf16[64,512]{1,0:T(8,128)(2,1)S(1)} %shard_map.82) | data formatting | bytes 131072
Async XLA Ops:
  0.0 0.7 %copy-start.6 = (s32[64,4]{0,1:T(4,128)S(1)}, s32[64,4]{0,1:T(4,128)}, u32[]{:S(2)}) copy-start(s32[64,4]{0,1:T(4,128)} %param.11) | copy-start | bytes 3076
  0.7 0.7 %copy-start.7 = (f32[64,4]{0,1:T(4,128)S(1)}, f32[64,4]{0,1:T(4,128)}, u32[]{:S(2)}) copy-start(f32[64,4]{0,1:T(4,128)} %param.12) | copy-start | bytes 3076
  1.4 0.7 %copy-start.4 = (f32[2048]{0:T(1024)S(1)}, f32[2048]{0:T(1024)}, u32[]{:S(2)}) copy-start(f32[2048]{0:T(1024)} %param.9) | copy-start | bytes 24580
  1.4 0.7 %copy-start.5 = (f32[2048]{0:T(1024)S(1)}, f32[2048]{0:T(1024)}, u32[]{:S(2)}) copy-start(f32[2048]{0:T(1024)} %param.10) | copy-start | bytes 24580
  2.1 1.2 %copy-start = (bf16[2,2048,128]{2,1,0:T(8,128)(2,1)S(1)}, bf16[2,2048,128]{2,1,0:T(8,128)(2,1)}, u32[]{:S(2)}) copy-start(bf16[2,2048,128]{2,1,0:T(8,128)(2,1)} %wg_ref.1) | copy-start | bytes 3145732
  3.3 1.2 %copy-start.1 = (bf16[2,2048,128]{2,1,0:T(8,128)(2,1)S(1)}, bf16[2,2048,128]{2,1,0:T(8,128)(2,1)}, u32[]{:S(2)}) copy-start(bf16[2,2048,128]{2,1,0:T(8,128)(2,1)} %wu_ref.1) | copy-start | bytes 3145732
  4.5 1.2 %copy-start.2 = (bf16[2,128,2048]{2,1,0:T(8,128)(2,1)S(1)}, bf16[2,128,2048]{2,1,0:T(8,128)(2,1)}, u32[]{:S(2)}) copy-start(bf16[2,128,2048]{2,1,0:T(8,128)(2,1)} %wd_ref.1) | copy-start | bytes 3145732
  5.8 0.9 %copy-start.3 = (bf16[64,2048]{1,0:T(8,128)(2,1)S(1)}, bf16[64,2048]{1,0:T(8,128)(2,1)}, u32[]{:S(2)}) copy-start(bf16[64,2048]{1,0:T(8,128)(2,1)} %tok_ref.1) | copy-start | bytes 786436

commit v2 on v1

v2 whole, which is shorter than its diff:
```python
import functools

import jax
import jax.numpy as jnp
from jax import lax
from jax.experimental import pallas as pl
from jax.experimental.pallas import tpu as pltpu
from jax.sharding import PartitionSpec as P

GROUPS = 4
CORES = 2
STAGES = 2
LEVELS = 32000.0
EPSILON = 1e-05
MESH = pl.DeviceIdType.MESH


def kernel(
    ep_size, tp_size,
    tok_hbm, gain_hbm, shift_hbm, ids_hbm, gw_hbm, wg_ref, wu_ref, wd_ref, out_ref,
    tok_ref, gain_ref, shift_ref, ids_ref, gw_ref,
    x_buf, xs_buf, sel_buf, wall_buf, wr_buf, wcat, wdn, acc,
    r1_send, r1_recv, r1_own, q_send, q_recv, u_send, u_recv, f_send, f_recv,
    in_sem, w_sem, s1_s, s1_r, wt_s, wt_r, a_s, a_r, b_s, b_r,
    c1_s, c1_r, c2_s, c2_r, cu_s, cu_r, c3_s, c3_r,
):
    tok_rows, features = tok_ref.shape
    local, _, units = wg_ref.shape
    top_k = ids_ref.shape[0]
    members = ep_size // GROUPS
    rows_tp = tp_size // CORES
    group_size = local * members
    half = tok_rows // 2
    quarter = features // tp_size
    lanes = GROUPS * half
    parts, _, width = wcat.shape
    per_stage = GROUPS // STAGES
    rows = per_stage * half
    scale_lanes = u_send.shape[-1]

    e = lax.axis_index("ep")
    j = lax.axis_index("tp")
    gme, m = e // members, e % members
    y, c = j // CORES, j % CORES
    partner = {"ep": e, "tp": y * CORES + (1 - c)}
    others = [(dm, dy) for dy in reversed(range(rows_tp)) for dm in reversed(range(members)) if dm or dy]
    chunk_of = {at: k for k, at in enumerate(others)}
    own = len(others)
    chunk_of[0, 0] = own

    def ahead(dm, dy):
        return lax.rem(m + dm, members), lax.rem(y + dy, rows_tp)

    def behind(dm, dy):
        return lax.rem(m + members - dm, members), lax.rem(y + rows_tp - dy, rows_tp)

    def member(dm, dy):
        mm, yy = ahead(dm, dy)
        return {"ep": gme * members + mm, "tp": yy * CORES + c}

    def block_at(db):
        return lax.rem(gme + GROUPS - db, GROUPS)

    def remote(src, dst, ssem, rsem, dev):
        return pltpu.make_async_remote_copy(
            src_ref=src, dst_ref=dst, send_sem=ssem, recv_sem=rsem,
            device_id=dev, device_id_type=MESH,
        )

    sent = []

    def start(*args):
        copy = remote(*args)
        copy.start()
        sent.append(copy)

    def arrive(slot, ssem, rsem):
        remote(slot, slot, ssem, rsem, partner).wait_recv()

    inputs = [
        pltpu.make_async_copy(s, d, in_sem.at[i])
        for i, (s, d) in enumerate([
            (ids_hbm, ids_ref), (gw_hbm, gw_ref), (tok_hbm, tok_ref),
            (gain_hbm, gain_ref), (shift_hbm, shift_ref),
        ])
    ]
    for copy in inputs:
        copy.start()

    barrier = pltpu.get_barrier_semaphore()
    greeted = 0
    for d in range(1, ep_size):
        pl.semaphore_signal(
            barrier, inc=1, device_id={"ep": lax.rem(e + d, ep_size), "tp": j}, device_id_type=MESH
        )
        greeted += 1
    for dm, dy in others:
        if dy:
            pl.semaphore_signal(barrier, inc=1, device_id=member(dm, dy), device_id_type=MESH)
            greeted += 1
    pl.semaphore_signal(barrier, inc=1, device_id=partner, device_id_type=MESH)
    greeted += 1

    weights = []
    for le in range(local):
        for source, at in ((wg_ref, 2 * le * units), (wu_ref, (2 * le + 1) * units)):
            weights.append(
                (source.at[le], wcat.at[at // width, :, pl.ds(at % width, units)])
            )
        for q in range(tp_size):
            weights.append((wd_ref.at[le, :, pl.ds(q * quarter, quarter)], wdn.at[q, le]))
    weights = [pltpu.make_async_copy(s, d, w_sem.at[i]) for i, (s, d) in enumerate(weights)]
    for copy in weights:
        copy.start()

    for copy in inputs[:2]:
        copy.wait()
    square = (tok_rows, tok_rows)
    token_at = lax.broadcasted_iota(jnp.int32, square, 0)
    other_at = lax.broadcasted_iota(jnp.int32, square, 1)
    ids = [
        jnp.sum(jnp.where(token_at == other_at, ids_ref[k : k + 1, :], 0), axis=1, keepdims=True)
        for k in range(top_k)
    ]
    gw = [
        jnp.sum(jnp.where(token_at == other_at, gw_ref[k : k + 1, :], 0.0), axis=1, keepdims=True)
        for k in range(top_k)
    ]
    group_of = ids[0] // group_size
    lane = lax.broadcasted_iota(jnp.int32, (tok_rows, lanes), 1)
    in_group = group_of == lane // half
    rank = jnp.dot(
        (other_at < token_at).astype(jnp.float32).astype(jnp.bfloat16),
        in_group.astype(jnp.float32).astype(jnp.bfloat16),
        preferred_element_type=jnp.float32,
    )
    picked = in_group & (rank == (lane % half).astype(jnp.float32))
    sel = picked.astype(jnp.float32)
    sel_bf = sel.astype(jnp.bfloat16)
    sel_buf[...] = sel_bf

    for copy in inputs[2:]:
        copy.wait()
    values = tok_ref[...].astype(jnp.float32)
    centre = jnp.mean(values, axis=-1, keepdims=True)
    spread = jnp.mean(jnp.square(values - centre), axis=-1, keepdims=True)
    share = pl.ds(pl.multiple_of(j * quarter, quarter), quarter)
    part = tok_ref[:, share].astype(jnp.float32)
    normed = (
        (part - centre) * lax.rsqrt(spread + EPSILON) * gain_ref[:, share] + shift_ref[:, share]
    ).astype(jnp.bfloat16)
    packed = lax.dot_general(
        sel_bf, normed, (((0,), (0,)), ((), ())), preferred_element_type=jnp.float32
    ).astype(jnp.bfloat16)
    xs_buf[...] = packed.reshape(GROUPS, half, quarter)

    pl.semaphore_wait(barrier, greeted)

    for dg in range(1, GROUPS):
        g = lax.rem(gme + dg, GROUPS)
        start(
            xs_buf.at[g], x_buf.at[m, j, dg], s1_s.at[dg], s1_r.at[dg],
            {"ep": g * members + m, "tp": j},
        )
    x_buf[m, j, 0] = xs_buf[gme]

    def spread_block(db):
        mine = x_buf.at[m, j, db]
        for k, (dm, dy) in enumerate(others):
            start(mine, mine, a_s.at[db, k], a_r.at[db, k], member(dm, dy))
        start(mine, mine, b_s.at[db, own], b_r.at[db, own], partner)

    spread_block(0)
    wall_buf[...] = jnp.zeros_like(wall_buf)
    for i in range(group_size):
        mine = 0.0
        for k in range(top_k):
            mine = mine + jnp.where(ids[k] - group_of * group_size == i, gw[k], 0.0)
        wall_buf[i : i + 1, :] = jnp.sum(sel * mine, axis=0, keepdims=True)
    for d in range(1, ep_size):
        start(
            wall_buf, wr_buf.at[e], wt_s.at[d], wt_r.at[d],
            {"ep": lax.rem(e + d, ep_size), "tp": j},
        )
    wr_buf[e] = wall_buf[...]
    for db in range(1, GROUPS):
        arrive(x_buf.at[m, j, db], s1_s.at[db], s1_r.at[db])
        spread_block(db)

    slot_row = lax.broadcasted_iota(jnp.int32, (half, lanes), 0) + gme * half
    diagonal = slot_row == lax.broadcasted_iota(jnp.int32, (half, lanes), 1)
    scale_eye = (
        lax.broadcasted_iota(jnp.int32, (rows, scale_lanes), 0)
        == lax.broadcasted_iota(jnp.int32, (rows, scale_lanes), 1)
    )

    def project(jj, blocks):
        held = [
            x_buf[lax.rem(m + dm, members), jj, db] for dm in range(members) for db in blocks
        ]
        held = jnp.concatenate(held, axis=0)
        depth = pl.ds(pl.multiple_of(jj * quarter, quarter), quarter)
        for part in range(parts):
            acc[part] += jnp.dot(held, wcat[part, depth, :], preferred_element_type=jnp.float32)

    def forward(blocks):
        for db in blocks:
            for k, at in enumerate(others):
                mm, yy = behind(*at)
                slot = x_buf.at[mm, yy * CORES + c, db]
                arrive(slot, a_s.at[db, k], a_r.at[db, k])
                start(slot, slot, b_s.at[db, k], b_r.at[db, k], partner)

    def experts(st, blocks):
        if st == 0:
            for copy in weights:
                copy.wait()
        acc[...] = jnp.zeros_like(acc)
        for dy in range(rows_tp):
            project(lax.rem(y + rows_tp - dy, rows_tp) * CORES + c, blocks)
        if st == 0:
            for d in range(1, ep_size):
                arrive(wr_buf.at[lax.rem(e + ep_size - d, ep_size)], wt_s.at[d], wt_r.at[d])
        for dy in range(rows_tp):
            for dm in range(members):
                mm, yy = behind(dm, dy)
                for db in blocks:
                    k = chunk_of[dm, dy]
                    slot = x_buf.at[mm, yy * CORES + (1 - c), db]
                    arrive(slot, b_s.at[db, k], b_r.at[db, k])
            project(lax.rem(y + rows_tp - dy, rows_tp) * CORES + (1 - c), blocks)
        hidden, scale = [], []
        for le in range(local):
            at, to = 2 * le * units, (2 * le + 1) * units
            gate = acc[at // width, :, at % width : at % width + units]
            up = acc[to // width, :, to % width : to % width + units]
            hidden.append((gate / (1.0 + jnp.exp(-gate)) * up).astype(jnp.bfloat16))
            columns = []
            for dm in range(members):
                for db in blocks:
                    source = block_at(db) * members + lax.rem(m + dm, members)
                    row = wr_buf[source, pl.ds(m * local + le, 1), :]
                    columns.append(jnp.sum(jnp.where(diagonal, row, 0.0), axis=1, keepdims=True))
            scale.append(jnp.concatenate(columns, axis=0))

        def lower(q):
            total = None
            for le in range(local):
                term = scale[le] * jnp.dot(
                    hidden[le], wdn[q, le], preferred_element_type=jnp.float32
                )
                total = term if total is None else total + term
            return total

        for dy in reversed(range(rows_tp)):
            q = lax.rem(y + dy, rows_tp) * CORES
            r1_send[st, dy] = lower(q + (1 - c))
            start(
                r1_send.at[st, dy], r1_recv.at[st, dy], c1_s.at[st, dy], c1_r.at[st, dy], partner
            )
        for dy in reversed(range(rows_tp)):
            q = lax.rem(y + dy, rows_tp) * CORES
            r1_own[st, dy] = lower(q + c)

    def summed(st, dm, dy):
        at = pl.ds(dm * rows, rows)
        return r1_own[st, dy, at, :] + r1_recv[st, dy, at, :]

    def reduce_send(st):
        for dy in reversed(range(rows_tp)):
            arrive(r1_recv.at[st, dy], c1_s.at[st, dy], c1_r.at[st, dy])
            for dm in reversed(range(members)):
                if not (dm or dy):
                    continue
                k = chunk_of[dm, dy]
                value = summed(st, dm, dy)
                top = jnp.maximum(jnp.max(jnp.abs(value), axis=1, keepdims=True), 1e-30)
                code = jnp.round(value * (LEVELS / top)).astype(jnp.int32).astype(jnp.int16)
                q_send[st, k] = code.reshape(per_stage, half, quarter)
                step = jnp.sum(
                    jnp.where(scale_eye, top * (1.0 / LEVELS), 0.0), axis=0, keepdims=True
                )
                u_send[st, k] = jnp.broadcast_to(step, u_send.shape[2:])
                start(
                    u_send.at[st, k], u_recv.at[st, k], cu_s.at[st, k], cu_r.at[st, k],
                    member(dm, dy),
                )
                for i in range(per_stage):
                    start(
                        q_send.at[st, k, i], q_recv.at[st, k, i],
                        c2_s.at[st, k, i], c2_r.at[st, k, i], member(dm, dy),
                    )

    def reduce_recv(st, blocks):
        total = summed(st, 0, 0)
        steps = []
        for k in range(own):
            arrive(u_recv.at[st, k], cu_s.at[st, k], cu_r.at[st, k])
            row = u_recv[st, k, 0:1, :]
            steps.append(jnp.sum(jnp.where(scale_eye, row, 0.0), axis=1, keepdims=True))
        for i, db in enumerate(blocks):
            at = slice(i * half, (i + 1) * half)
            block = total[at]
            for k in range(own):
                arrive(q_recv.at[st, k, i], c2_s.at[st, k, i], c2_r.at[st, k, i])
                code = q_recv[st, k, i].astype(jnp.int32).astype(jnp.float32)
                block = block + code * steps[k][at]
            f_send[db] = block.astype(jnp.bfloat16)
            if db:
                start(
                    f_send.at[db], f_recv.at[gme], c3_s.at[db], c3_r.at[db],
                    {"ep": block_at(db) * members + m, "tp": j},
                )
            else:
                f_recv[gme] = f_send[0]

    stages = [range(st * per_stage, (st + 1) * per_stage) for st in range(STAGES)]
    for st, blocks in enumerate(stages):
        forward(blocks)
        experts(st, blocks)
        if st:
            reduce_send(st)
            reduce_recv(st - 1, stages[st - 1])
        else:
            reduce_send(st)
    reduce_recv(STAGES - 1, stages[-1])
    for db in range(1, GROUPS):
        arrive(f_recv.at[lax.rem(gme + db, GROUPS)], c3_s.at[db], c3_r.at[db])
    out_ref[...] = jnp.dot(
        sel_buf[...], f_recv[...].reshape(lanes, quarter), preferred_element_type=jnp.float32
    ).astype(jnp.bfloat16)
    for copy in sent:
        copy.wait_send()


def per_device(tokens, norm_gain, norm_shift, expert_ids, gate_weights, w_gate, w_up, w_down):
    ep_size, tp_size = lax.axis_size("ep"), lax.axis_size("tp")
    tok_rows, features = tokens.shape
    local, _, units = w_gate.shape
    members, rows_tp = ep_size // GROUPS, tp_size // CORES
    half, quarter = tok_rows // 2, features // tp_size
    lanes = GROUPS * half
    group_size = local * members
    padded = -(-group_size // 8) * 8
    chunks = members * rows_tp
    parts, width = (1, 2 * local * units) if units % 128 == 0 else (2 * local, units)
    bf16, f32 = jnp.bfloat16, jnp.float32
    dma = pltpu.SemaphoreType.DMA
    vmem = pl.BlockSpec(memory_space=pltpu.VMEM)
    hbm = pl.BlockSpec(memory_space=pltpu.MemorySpace.HBM)
    per_stage = GROUPS // STAGES
    rows = per_stage * half
    all_rows = members * rows
    scale_lanes = -(-rows // 128) * 128
    return pl.pallas_call(
        functools.partial(kernel, ep_size, tp_size),
        out_shape=jax.ShapeDtypeStruct((tok_rows, quarter), bf16),
        in_specs=[hbm] * 8,
        out_specs=vmem,
        scratch_shapes=[
            pltpu.VMEM((tok_rows, features), bf16),
            pltpu.VMEM((1, features), f32),
            pltpu.VMEM((1, features), f32),
            pltpu.VMEM((expert_ids.shape[1], tok_rows), jnp.int32),
            pltpu.VMEM((expert_ids.shape[1], tok_rows), f32),
            pltpu.VMEM((members, tp_size, GROUPS, half, quarter), bf16),
            pltpu.VMEM((GROUPS, half, quarter), bf16),
            pltpu.VMEM((tok_rows, lanes), bf16),
            pltpu.VMEM((padded, lanes), f32),
            pltpu.VMEM((ep_size, padded, lanes), f32),
            pltpu.VMEM((parts, features, width), bf16),
            pltpu.VMEM((tp_size, local, units, quarter), bf16),
            pltpu.VMEM((parts, all_rows, width), f32),
            pltpu.VMEM((STAGES, rows_tp, all_rows, quarter), f32),
            pltpu.VMEM((STAGES, rows_tp, all_rows, quarter), f32),
            pltpu.VMEM((STAGES, rows_tp, all_rows, quarter), f32),
            pltpu.VMEM((STAGES, chunks - 1, per_stage, half, quarter), jnp.int16),
            pltpu.VMEM((STAGES, chunks - 1, per_stage, half, quarter), jnp.int16),
            pltpu.VMEM((STAGES, chunks - 1, 8, scale_lanes), f32),
            pltpu.VMEM((STAGES, chunks - 1, 8, scale_lanes), f32),
            pltpu.VMEM((GROUPS, half, quarter), bf16),
            pltpu.VMEM((GROUPS, half, quarter), bf16),
            dma((5,)),
            dma((local * (2 + tp_size),)),
            dma((GROUPS,)), dma((GROUPS,)),
            dma((ep_size,)), dma((ep_size,)),
            dma((GROUPS, chunks)), dma((GROUPS, chunks)),
            dma((GROUPS, chunks)), dma((GROUPS, chunks)),
            dma((STAGES, rows_tp)), dma((STAGES, rows_tp)),
            dma((STAGES, chunks, per_stage)), dma((STAGES, chunks, per_stage)),
            dma((STAGES, chunks)), dma((STAGES, chunks)),
            dma((GROUPS,)), dma((GROUPS,)),
        ],
        compiler_params=pltpu.CompilerParams(
            collective_id=0, has_side_effects=True, vmem_limit_bytes=60 * 1024 * 1024
        ),
    )(
        tokens, norm_gain.reshape(1, features), norm_shift.reshape(1, features),
        expert_ids.T, gate_weights.T, w_gate, w_up, w_down,
    )


def solution(mesh):
    return jax.shard_map(
        per_device,
        mesh=mesh,
        in_specs=(
            P("ep", None),
            P(),
            P(),
            P("ep", None),
            P("ep", None),
            P("ep", None, "tp"),
            P("ep", None, "tp"),
            P("ep", "tp", None),
        ),
        out_specs=P("ep", "tp"),
        check_vma=False,
    )
```

time: 45.7 us -> 32.2 us (0.70)
  Pallas kernels: 38 us -> 30.5 us
  local copies, waits for them, and re-layouts: 7.33 us -> 1.47 us
    pallas_call x1, Pallas kernels: 38 us -> 30.5 us  [per_device(): pl.pallas_call(functools.partial(kernel, ep_size, tp_size), out_shape=jax...]
    unnamed x19 -> x1, local copies, waits for them, and re-layouts: 7.33 us -> 1.47 us
where the time goes in v2:
time: 32.2 us; the launch traced here: 32 us
  Pallas kernels  30.5 us (95%)
  local copies, waits for them, and re-layouts  1.47 us (5%)
    pallas_call x1, Pallas kernels, per_device(): pl.pallas_call(functools.partial(kernel, ep_size, tp_size), out_shape=jax...  30.5 us
    unnamed x1, local copies, waits for them, and re-layouts  1.47 us

profile of v2, /device:TPU:0, one launch (start us, length us, event | category | flops | bytes accessed | tf_op | source)
XLA Modules:
  0.0 32.0 jit_solution(3077903470666175236)
XLA Ops:
  0.0 30.5 %shard_map.82 = bf16[64,512]{1,0:T(8,128)(2,1)} custom-call(bf16[64,2048]{1,0:T(8,128)(2,1)} %tok_hbm.1, f32[1,2048]{1,0:T(1,128)} %bitcast.4, f32[1,2048]{1,0:T(1,128)} %bitcast.5, s32[4,64]{1,0:T(4,128)} %bitcast.6, f32[4,64]{1,0:T(4,128)} %bitcast.7, bf16[2,2048,128]{2,1,0:T(8,128)(2,1)} %wg_ref.1, bf16[2,2048,128]{2,1,0:T(8,128)(2,1)} %wu_ref.1, ...), custom_call_target="tpu_custom_call" | custom-call | tf_op jit(solution)/shard_map/pallas_call | solution.py:355
  30.5 1.5 %copy.10 = bf16[64,512]{1,0:T(8,128)(2,1)} copy(bf16[64,512]{1,0:T(8,128)(2,1)} %shard_map.82) | data formatting | bytes 131072

commit v3 on v2

--- a/solution.py
+++ b/solution.py
@@ -315,14 +315,14 @@
                 f_recv[gme] = f_send[0]
 
     stages = [range(st * per_stage, (st + 1) * per_stage) for st in range(STAGES)]
+    forward(stages[0])
     for st, blocks in enumerate(stages):
-        forward(blocks)
         experts(st, blocks)
+        if st + 1 < STAGES:
+            forward(stages[st + 1])
+        reduce_send(st)
         if st:
-            reduce_send(st)
             reduce_recv(st - 1, stages[st - 1])
-        else:
-            reduce_send(st)
     reduce_recv(STAGES - 1, stages[-1])
     for db in range(1, GROUPS):
         arrive(f_recv.at[lax.rem(gme + db, GROUPS)], c3_s.at[db], c3_r.at[db])

time: 32.2 us -> 31.3 us (0.972)
  Pallas kernels: 30.5 us -> 29.7 us
    pallas_call x1, Pallas kernels: 30.5 us -> 29.7 us  [per_device(): pl.pallas_call(functools.partial(kernel, ep_size, tp_size), out_shape=jax...]
where the time goes in v3:
time: 31.3 us; the launch traced here: 31.1 us
  Pallas kernels  29.7 us (95%)
  local copies, waits for them, and re-layouts  1.47 us (5%)
    pallas_call x1, Pallas kernels, per_device(): pl.pallas_call(functools.partial(kernel, ep_size, tp_size), out_shape=jax...  29.7 us
    unnamed x1, local copies, waits for them, and re-layouts  1.47 us

profile of v3, /device:TPU:0, one launch (start us, length us, event | category | flops | bytes accessed | tf_op | source)
XLA Modules:
  0.0 31.1 jit_solution(10187927015733535509)
XLA Ops:
  0.0 29.7 %shard_map.82 = bf16[64,512]{1,0:T(8,128)(2,1)} custom-call(bf16[64,2048]{1,0:T(8,128)(2,1)} %tok_hbm.1, f32[1,2048]{1,0:T(1,128)} %bitcast.4, f32[1,2048]{1,0:T(1,128)} %bitcast.5, s32[4,64]{1,0:T(4,128)} %bitcast.6, f32[4,64]{1,0:T(4,128)} %bitcast.7, bf16[2,2048,128]{2,1,0:T(8,128)(2,1)} %wg_ref.1, bf16[2,2048,128]{2,1,0:T(8,128)(2,1)} %wu_ref.1, ...), custom_call_target="tpu_custom_call" | custom-call | tf_op jit(solution)/shard_map/pallas_call | solution.py:355
  29.7 1.5 %copy.10 = bf16[64,512]{1,0:T(8,128)(2,1)} copy(bf16[64,512]{1,0:T(8,128)(2,1)} %shard_map.82) | data formatting | bytes 131072
